TPU v7x, 32 devices: a whole 2x2x4 slice. The times are simulated.
32 devices in a mesh: grp: 2 (over y), sp: 4 (over z), tp: 4 (over x, core).
Axes of the slice: x: 2, y: 2, z: 4, core: 2. Of those that a mesh axis runs over, the one named last changes fastest.
Arguments:
- stream: bfloat16 [6144, 4096], P(('grp', 'sp'), 'tp'), parts along dimension 0, may hold values from -400 to 400
- in_weight: bfloat16 [2, 1024, 4096], P(None, 'sp', 'tp'), may hold values from -0.09375 to 0.09375
- out_weight: bfloat16 [2, 1024, 4096], P(None, 'sp', 'tp'), may hold values from -0.1875 to 0.1875
- group_mix: bfloat16 [2, 4, 256, 256], replicated, may hold values from -0.375 to 0.375
- pool_gain: float32 [2, 1024], replicated, may hold values from 0.1 to 1.9
- norm_gain: float32 [2, 4096], P(None, 'tp'), may hold values from 0.1 to 1.9
- norm_shift: float32 [2, 4096], P(None, 'tp'), may hold values from -3 to 3
Outputs:
- refined: bfloat16 [6144, 4096], P(('grp', 'sp'), 'tp'), parts along dimension 0
There are 2 independent parts, one for each index of `grp`. A program takes and returns all parts, laid end to end along the dimension named above; an argument that names none is the same for every part. Nothing has to cross between parts.
All inputs are finite; a program needn't handle non-finite values.
Results may differ from a plain program's by a relative error of at most 0.015.
Values may be sent and summed in bfloat16 or wider, within the bound.
A program may use at most 64 MiB of HBM per device.

v0:
```python
import jax
import jax.numpy as jnp
from jax import lax
from jax.sharding import PartitionSpec as P

D = 4096
POOL = 1024
GROUPS = 4
GROUP_WIDTH = 256
LAYERS = 2
epsilon = 1e-05


def passed_along(block, axis, distance):
    devices = range(lax.axis_size(axis))
    route = [(i - distance, i) for i in devices if i - distance in devices]
    return lax.ppermute(block, axis, route)


def pooled_windows(hidden, tok_start):
    reach = 2**GROUPS - 1
    length = hidden.shape[1]
    channels = hidden.shape[0]
    earlier = passed_along(hidden[:, length - reach :], "sp", 1)
    extended = jnp.concatenate([earlier, hidden], axis=1).astype(jnp.float32)
    group_ids = (jnp.arange(channels, dtype=jnp.int32) // GROUP_WIDTH)[:, None]
    running = extended
    window_sums = jnp.zeros((channels, length), jnp.float32)
    for octave in range(GROUPS):
        offset = 2**octave
        running = running[:, offset:] + running[:, : running.shape[1] - offset]
        window_sums = jnp.where(
            group_ids == octave, running[:, running.shape[1] - length :], window_sums
        )
    positions = (tok_start + jnp.arange(length, dtype=jnp.int32) + 1).astype(jnp.float32)
    widths = jnp.exp2((group_ids + 1).astype(jnp.float32))
    counts = jnp.minimum(positions[None, :], widths)
    return (window_sums / counts - hidden.astype(jnp.float32)).astype(jnp.bfloat16)


def per_device(stream, in_weight, out_weight, group_mix, pool_gain, norm_gain, norm_shift):
    tok_rows = stream.shape[0]
    tok_start = lax.axis_index("sp") * tok_rows
    alpha = (2.0 * LAYERS) ** 0.25
    contract_rows = (((0,), (0,)), ((), ()))
    contract_cols = (((1,), (1,)), ((), ()))
    current = stream
    for layer_index in range(LAYERS):
        whole_in = lax.all_gather(in_weight[layer_index], "sp", axis=0, tiled=True)
        partial_value = lax.dot_general(
            whole_in, current, contract_cols, preferred_element_type=jnp.float32
        )
        hidden = lax.psum(partial_value.astype(jnp.bfloat16), "tp")
        pooled = pooled_windows(hidden, tok_start)
        grouped = pooled.reshape(GROUPS, GROUP_WIDTH, tok_rows)
        mixed = jnp.einsum(
            "gio,git->got", group_mix[layer_index], grouped, preferred_element_type=jnp.float32
        )
        gains = pool_gain[layer_index].reshape(GROUPS, GROUP_WIDTH, 1)
        scaled = (mixed * gains).astype(jnp.bfloat16).reshape(POOL, tok_rows)
        branch = lax.dot_general(
            scaled,
            lax.all_gather(out_weight[layer_index], "sp", axis=0, tiled=True),
            contract_rows,
            preferred_element_type=jnp.float32,
        )
        summed = alpha * current.astype(jnp.float32) + branch
        row_sum, row_squares = lax.psum(
            (jnp.sum(summed, axis=1), jnp.sum(summed * summed, axis=1)), "tp"
        )
        row_mean = row_sum / D
        row_var = row_squares / D - row_mean * row_mean
        normed = (summed - row_mean[:, None]) * lax.rsqrt(row_var + epsilon)[:, None]
        current = (
            normed * norm_gain[layer_index][None, :] + norm_shift[layer_index][None, :]
        ).astype(jnp.bfloat16)
    return current


def solution(mesh):
    in_specs = (
        P(("grp", "sp"), "tp"),
        P(None, "sp", "tp"),
        P(None, "sp", "tp"),
        P(),
        P(),
        P(None, "tp"),
        P(None, "tp"),
    )
    out_specs = P(("grp", "sp"), "tp")
    return jax.shard_map(
        per_device, mesh=mesh, in_specs=in_specs, out_specs=out_specs, check_vma=False
    )
```

profile of v0, /device:TPU:0, one launch (start us, length us, event | category | flops | bytes accessed | tf_op | source)
XLA Modules:
  0.0 312.8 jit_solution(13905823871252964514)
XLA Ops:
  6.5 2.2 fusion.49
  8.9 48.5 %all-gather.9.cloned.1.call-done = bf16[1,1024,1024]{2,1,0:T(8,128)(2,1)} async-done(((bf16[1,256,1024]{2,1,0:T(8,128)(2,1)}), bf16[1,1024,1024]{2,1,0:T(8,128)(2,1)}) %all-gather.9.cloned.1.call-update) | async-done | bytes 2097168 | tf_op jit(solution)/shard_map/all_gather | solution.py:49
  57.3 5.0 %fusion.22 = bf16[1024,768]{1,0:T(8,128)(2,1)} fusion(bf16[768,1024]{1,0:T(8,128)(2,1)} %param.7, bf16[1,1024,1024]{2,1,0:T(8,128)(2,1)} %all-gather.9.cloned.1.call-done), kind=kOutput, calls=%fused_computation.40 | convolution fusion | flops 1611399168 | bytes 5242880 | tf_op jit(solution)/shard_map/dot_general | solution.py:50
  62.4 1.1 fusion.48
  64.3 39.9 %all-reduce.5.cloned.1.call-done = bf16[1024,768]{1,0:T(8,128)(2,1)} async-done(((bf16[1024,768]{1,0:T(8,128)(2,1)}), bf16[1024,768]{1,0:T(8,128)(2,1)}) %all-reduce.5.cloned.1.call-update) | async-done | bytes 1572880 | tf_op jit(solution)/shard_map/psum | solution.py:53
  104.2 1.1 slice.138
  105.3 3.4 %collective-permute-start = (bf16[1024,15]{1,0:T(8,128)(2,1)S(1)}, bf16[1024,15]{1,0:T(8,128)(2,1)S(1)}, u32[]{:S(2)}, u32[]{:S(2)}) collective-permute-start(bf16[1024,15]{1,0:T(8,128)(2,1)S(1)} %slice.138), channel_id=1, source_target_pairs={{0,4},{4,8},{8,12},{1,5},{5,9},{9,13},{2,6},{6,10},{10,14},{3,7},{... | collective-permute-start | bytes 92168 | tf_op jit(solution)/shard_map/ppermute | solution.py:17
  108.7 5.4 %collective-permute-done = bf16[1024,15]{1,0:T(8,128)(2,1)S(1)} collective-permute-done((bf16[1024,15]{1,0:T(8,128)(2,1)S(1)}, bf16[1024,15]{1,0:T(8,128)(2,1)S(1)}, u32[]{:S(2)}, u32[]{:S(2)}) %collective-permute-start) | collective-permute-done | bytes 30752 | tf_op jit(solution)/shard_map/ppermute | solution.py:17
  114.1 2.3 maximum_convert_fusion
  116.4 1.0 slice_add_fusion.5
  117.4 1.0 slice_add_fusion.4
  118.5 1.0 slice_add_fusion.3
  119.9 4.1 %fusion.1 = bf16[1024,768]{1,0:T(8,128)(2,1)S(1)} fusion(f32[1024,782]{1,0:T(8,128)S(1)} %slice_add_fusion.5, f32[1024,780]{1,0:T(8,128)S(1)} %slice_add_fusion.4, f32[1024,776]{1,0:T(8,128)S(1)} %slice_add_fusion.3, bf16[1024,768]{1,0:T(8,128)(2,1)S(1)} %copy-done, f32[1024]{0:T(1024)S(1)} %fusion.44, f32[768]{0:T(1024)S(1)} %add_convert_fusion.2, ...), kind=kLoop, calls=%fused_computation.9 | loop fusion | flops 7864320 | bytes 15739904 | tf_op jit(solution)/shard_map/convert_element_type | solution.py:38
  124.7 26.8 %all-gather.11.cloned.1.call-done = bf16[1,1024,1024]{2,1,0:T(8,128)(2,1)} async-done(((bf16[1,256,1024]{2,1,0:T(8,128)(2,1)}), bf16[1,1024,1024]{2,1,0:T(8,128)(2,1)}) %all-gather.11.cloned.1.call-update) | async-done | bytes 2097168 | tf_op jit(solution)/shard_map/all_gather | solution.py:63
  151.5 5.8 %fusion.47 = (f32[768]{0:T(1024)S(1)}, f32[768]{0:T(1024)S(1)}, f32[768,1024]{1,0:T(8,128)}) fusion(bf16[1024,768]{1,0:T(8,128)(2,1)S(1)} %bitcast.56, bf16[1,1024,1024]{2,1,0:T(8,128)(2,1)} %all-gather.11.cloned.1.call-done, bf16[768,1024]{1,0:T(8,128)(2,1)} %param.7), kind=kOutput, calls=%fused_computation.70 | convolution fusion | flops 1615329792 | bytes 8394752 | tf_op jit(solution)/shard_map/dot_general | solution.py:61
  157.3 6.5 %all-reduce.1 = (f32[768]{0:T(1024)S(1)}, f32[768]{0:T(1024)S(1)}) all-reduce(f32[768]{0:T(1024)S(1)} %get-tuple-element.8, f32[768]{0:T(1024)S(1)} %get-tuple-element.7), channel_id=1, replica_groups=mesh['grp'=2,'sp'=4,'tp'=4] {'tp'}, use_global_device_ids=true, to_apply=%region_4.5 | all-reduce | flops 1536 | bytes 12288 | tf_op jit(solution)/shard_map/psum | solution.py:68
  163.8 33.6 %all-gather.13.cloned.1.call-done = bf16[1,1024,1024]{2,1,0:T(8,128)(2,1)} async-done(((bf16[1,256,1024]{2,1,0:T(8,128)(2,1)}), bf16[1,1024,1024]{2,1,0:T(8,128)(2,1)}) %all-gather.13.cloned.1.call-update) | async-done | bytes 2097168 | tf_op jit(solution)/shard_map/all_gather | solution.py:49
  197.4 5.6 %fusion.28 = bf16[1024,768]{1,0:T(8,128)(2,1)} fusion(bf16[1,1024,1024]{2,1,0:T(8,128)(2,1)} %all-gather.13.cloned.1.call-done, f32[768,1024]{1,0:T(8,128)} %get-tuple-element.27, f32[1024]{0:T(1024)S(1)} %bitcast.61, f32[1024]{0:T(1024)S(1)} %bitcast.59, f32[768]{0:T(1024)S(1)} %get-tuple-element.26, f32[768]{0:T(1024)S(1)} %get-tuple-element.25), kind=kOutput, calls=%fused_computation.42 | convolution fusion | flops 1615331328 | bytes 6830080 | tf_op jit(solution)/shard_map/dot_general | solution.py:50
  203.7 41.2 %all-reduce.7.cloned.1.call-done = bf16[1024,768]{1,0:T(8,128)(2,1)} async-done(((bf16[1024,768]{1,0:T(8,128)(2,1)}), bf16[1024,768]{1,0:T(8,128)(2,1)}) %all-reduce.7.cloned.1.call-update) | async-done | bytes 1572880 | tf_op jit(solution)/shard_map/psum | solution.py:53
  244.9 1.1 slice.149
  246.0 3.6 %collective-permute-start.1 = (bf16[1024,15]{1,0:T(8,128)(2,1)S(1)}, bf16[1024,15]{1,0:T(8,128)(2,1)S(1)}, u32[]{:S(2)}, u32[]{:S(2)}) collective-permute-start(bf16[1024,15]{1,0:T(8,128)(2,1)S(1)} %slice.149), channel_id=1, source_target_pairs={{0,4},{4,8},{8,12},{1,5},{5,9},{9,13},{2,6},{6,10},{10,14},{3,7},{... | collective-permute-start | bytes 92168 | tf_op jit(solution)/shard_map/ppermute | solution.py:17
  249.6 5.5 %collective-permute-done.1 = bf16[1024,15]{1,0:T(8,128)(2,1)S(1)} collective-permute-done((bf16[1024,15]{1,0:T(8,128)(2,1)S(1)}, bf16[1024,15]{1,0:T(8,128)(2,1)S(1)}, u32[]{:S(2)}, u32[]{:S(2)}) %collective-permute-start.1) | collective-permute-done | bytes 30752 | tf_op jit(solution)/shard_map/ppermute | solution.py:17
  255.2 2.2 maximum_convert_fusion.1
  257.4 1.0 slice_add_fusion.2
  258.4 1.0 slice_add_fusion.1
  259.4 1.0 slice_add_fusion
  260.9 4.1 %fusion.3 = bf16[1024,768]{1,0:T(8,128)(2,1)S(1)} fusion(f32[1024,782]{1,0:T(8,128)S(1)} %slice_add_fusion.2, f32[1024,780]{1,0:T(8,128)S(1)} %slice_add_fusion.1, f32[1024,776]{1,0:T(8,128)S(1)} %slice_add_fusion, bf16[1024,768]{1,0:T(8,128)(2,1)S(1)} %copy-done.1, f32[1024]{0:T(1024)S(1)} %fusion.44, f32[768]{0:T(1024)S(1)} %add_convert_fusion.2, ...), kind=kLoop, calls=%fused_computation.11 | loop fusion | flops 7864320 | bytes 15739904 | tf_op jit(solution)/shard_map/convert_element_type | solution.py:38
  265.0 1.8 multiply_convert_fusion
  266.8 25.3 %all-gather.15.cloned.1.call-done = bf16[1,1024,1024]{2,1,0:T(8,128)(2,1)} async-done(((bf16[1,256,1024]{2,1,0:T(8,128)(2,1)}), bf16[1,1024,1024]{2,1,0:T(8,128)(2,1)}) %all-gather.15.cloned.1.call-update) | async-done | bytes 2097168 | tf_op jit(solution)/shard_map/all_gather | solution.py:63
  292.1 5.6 %fusion.46 = (f32[768]{0:T(1024)S(1)}, f32[768]{0:T(1024)S(1)}, f32[768,1024]{1,0:T(8,128)S(1)}) fusion(bf16[1024,768]{1,0:T(8,128)(2,1)} %bitcast.55, bf16[1,1024,1024]{2,1,0:T(8,128)(2,1)} %all-gather.15.cloned.1.call-done, f32[1024]{0:T(1024)S(1)} %bitcast.62, f32[1024]{0:T(1024)S(1)} %bitcast.60, f32[768]{0:T(1024)S(1)} %get-tuple-element.26, ...), kind=kOutput, calls=%fused_computation.69 | convolution fusion | flops 1619261952 | bytes 9981952 | tf_op jit(solution)/shard_map/dot_general | solution.py:61
  297.7 6.5 %all-reduce = (f32[768]{0:T(1024)S(1)}, f32[768]{0:T(1024)S(1)}) all-reduce(f32[768]{0:T(1024)S(1)} %get-tuple-element.6, f32[768]{0:T(1024)S(1)} %get-tuple-element.5), channel_id=1, replica_groups=mesh['grp'=2,'sp'=4,'tp'=4] {'tp'}, use_global_device_ids=true, to_apply=%region_9.10 | all-reduce | flops 1536 | bytes 12288 | tf_op jit(solution)/shard_map/psum | solution.py:68
  304.2 1.7 add_convert_fusion
  (38 shorter events, 2.9 us)
Async XLA Ops:
  6.5 50.8 %all-gather.9.cloned.1.call-start = ((), (), s32[]{:S(2)}) async-start(), calls=%async_computation.2 | async-start | bytes 2621440 | tf_op jit(solution)/shard_map/all_gather | solution.py:49
  8.8 53.6 %copy-start.2 = (bf16[2,256,1024]{2,1,0:T(8,128)(2,1)S(1)}, bf16[2,256,1024]{2,1,0:T(8,128)(2,1)}, u32[]{:S(2)}) copy-start(bf16[2,256,1024]{2,1,0:T(8,128)(2,1)} %param.9) | copy-start | bytes 3145732
  8.8 95.4 %all-reduce.5.cloned.1.call-start = ((), (), s32[]{:S(2)}) async-start(), calls=%async_computation | async-start | bytes 3145728 | tf_op jit(solution)/shard_map/psum | solution.py:53
  62.3 1.9 copy-start.4
  62.3 1.9 copy-start.5
  62.3 1.9 copy-start.6
  62.4 89.1 %all-gather.11.cloned.1.call-start = ((), (), s32[]{:S(2)}) async-start(), calls=%async_computation.3 | async-start | bytes 2621440 | tf_op jit(solution)/shard_map/all_gather | solution.py:63
  63.5 133.9 %all-gather.13.cloned.1.call-start = ((), (), s32[]{:S(2)}) async-start(), calls=%async_computation.4 | async-start | bytes 2621440 | tf_op jit(solution)/shard_map/all_gather | solution.py:49
  64.1 180.8 %all-reduce.7.cloned.1.call-start = ((), (), s32[]{:S(2)}) async-start(), calls=%async_computation.1 | async-start | bytes 3145728 | tf_op jit(solution)/shard_map/psum | solution.py:53
  105.3 8.8 %collective-permute-start = (bf16[1024,15]{1,0:T(8,128)(2,1)S(1)}, bf16[1024,15]{1,0:T(8,128)(2,1)S(1)}, u32[]{:S(2)}, u32[]{:S(2)}) collective-permute-start(bf16[1024,15]{1,0:T(8,128)(2,1)S(1)} %slice.138), channel_id=1, source_target_pairs={{0,4},{4,8},{8,12},{1,5},{5,9},{9,13},{2,6},{6,10},{10,14},{3,7},{... | collective-permute-start | bytes 92168 | tf_op jit(solution)/shard_map/ppermute | solution.py:17
  118.5 1.4 copy-start
  119.9 4.1 %copy-start.3 = (bf16[2,4,256,256]{3,2,1,0:T(8,128)(2,1)S(1)}, bf16[2,4,256,256]{3,2,1,0:T(8,128)(2,1)}, u32[]{:S(2)}) copy-start(bf16[2,4,256,256]{3,2,1,0:T(8,128)(2,1)} %param.10) | copy-start | bytes 3145732
  203.1 89.0 %all-gather.15.cloned.1.call-start = ((), (), s32[]{:S(2)}) async-start(), calls=%async_computation.5 | async-start | bytes 2621440 | tf_op jit(solution)/shard_map/all_gather | solution.py:63
  246.0 9.2 %collective-permute-start.1 = (bf16[1024,15]{1,0:T(8,128)(2,1)S(1)}, bf16[1024,15]{1,0:T(8,128)(2,1)S(1)}, u32[]{:S(2)}, u32[]{:S(2)}) collective-permute-start(bf16[1024,15]{1,0:T(8,128)(2,1)S(1)} %slice.149), channel_id=1, source_target_pairs={{0,4},{4,8},{8,12},{1,5},{5,9},{9,13},{2,6},{6,10},{10,14},{3,7},{... | collective-permute-start | bytes 92168 | tf_op jit(solution)/shard_map/ppermute | solution.py:17
  259.4 1.4 copy-start.1
Sparse Core Ops, SparseCore 0:
  8.9 48.3 all-gather.8
  62.5 41.6 all-reduce.4
  105.8 45.7 all-gather.10
  152.9 44.4 all-gather.12
  203.2 41.6 all-reduce.6
  246.3 45.7 all-gather.14
where the time goes:
time: 313 us
  waiting for transfers between devices  227 us (73%)
  matrix products  24.5 us (8%)
  other arithmetic  20.6 us (7%)
  between operations  13.7 us (4%)
  blocking collectives  13 us (4%)
  starting transfers between devices  7.2 us (2%)
  local copies, waits for them, and re-layouts  6.35 us (2%)
    all_gather x2, waiting for transfers between devices, per_device(): whole_in = lax.all_gather(in_weight[layer_index], 'sp', axis=0, tiled=True)  82.1 us
    psum x2, waiting for transfers between devices, per_device(): hidden = lax.psum(partial_value.astype(jnp.bfloat16), 'tp')  81.1 us
    all_gather x2, waiting for transfers between devices, per_device(): lax.all_gather(out_weight[layer_index], 'sp', axis=0, tiled=True)  52.2 us
    psum x2, blocking collectives, per_device(): lax.psum((jnp.sum(summed, axis=1), jnp.sum(summed * summed, axis=1)), 'tp')  13 us
    dot_general x2, matrix products, per_device(): lax.dot_general(scaled, lax.all_gather(out_weight[layer_index], 'sp', axi...  11.4 us
    ppermute x2, waiting for transfers between devices, passed_along(): return lax.ppermute(block, axis, route)  10.9 us
    dot_general x2, matrix products, per_device(): lax.dot_general(whole_in, current, contract_cols, preferred_element_type=...  10.6 us
    convert_element_type x2, other arithmetic, pooled_windows(): (window_sums / counts - hidden.astype(jnp.float32)).astype(jnp.bfloat16)  8.26 us
  transfers between devices with their start and end apart: 8, of which 8 were waited for; matrix products, arithmetic and copies ran while one was open for 10% of the time, Pallas kernels for 0%

commit v1 on v0

--- a/solution.py
+++ b/solution.py
@@ -46,7 +46,14 @@
     contract_cols = (((1,), (1,)), ((), ()))
     current = stream
     for layer_index in range(LAYERS):
-        whole_in = lax.all_gather(in_weight[layer_index], "sp", axis=0, tiled=True)
+        ring = [in_weight[layer_index]]
+        for hop in range(3):
+            ring.append(lax.ppermute(ring[-1], "sp", [(dev, (dev + 1) % 4) for dev in range(4)]))
+        whole_in = jnp.roll(
+            jnp.concatenate(ring[::-1], axis=0),
+            (lax.axis_index("sp") + 1) * ring[0].shape[0],
+            axis=0,
+        )
         partial_value = lax.dot_general(
             whole_in, current, contract_cols, preferred_element_type=jnp.float32
         )

time: 313 us -> 240 us (0.77)
  waiting for transfers between devices: 227 us -> 142 us
  matrix products: 24.5 us -> 30.7 us
  starting transfers between devices: 7.2 us -> 12.1 us
    all_gather x2 -> x0, waiting for transfers between devices: 82.1 us -> none  [per_device(): whole_in = lax.all_gather(in_weight[layer_index], 'sp', axis=0, tiled=True)]
    ppermute x0 -> x6, waiting for transfers between devices: none -> 55 us  [per_device(): lax.ppermute(ring[-1], 'sp', [(dev, (dev + 1) % 4) for dev in range(4)])]
    all_gather x2, waiting for transfers between devices: 52.2 us -> 0.03 us  [per_device(): lax.all_gather(out_weight[layer_index], 'sp', axis=0, tiled=True)]
    psum x2, waiting for transfers between devices: 81.1 us -> 70.6 us  [per_device(): hidden = lax.psum(partial_value.astype(jnp.bfloat16), 'tp')]
    dot_general x2, matrix products: 10.6 us -> 16.9 us  [per_device(): lax.dot_general(whole_in, current, contract_cols, preferred_element_type=...]
    ppermute x0 -> x6, starting transfers between devices: none -> 4.87 us  [per_device(): lax.ppermute(ring[-1], 'sp', [(dev, (dev + 1) % 4) for dev in range(4)])]
    ppermute x2, waiting for transfers between devices: 10.9 us -> 15.7 us  [passed_along(): return lax.ppermute(block, axis, route)]
  transfers between devices with their start and end apart: 8 -> 12, of which waited for: 8 -> 8; matrix products, arithmetic and copies ran while one was open for 10% -> 13% of each run, Pallas kernels for 0% -> 0%
where the time goes in v1:
time: 240 us; the launch traced here: 239 us
  waiting for transfers between devices  142 us (59%)
  matrix products  30.7 us (13%)
  other arithmetic  20.6 us (9%)
  between operations  15.1 us (6%)
  blocking collectives  13.4 us (6%)
  starting transfers between devices  12.1 us (5%)
  local copies, waits for them, and re-layouts  5.33 us (2%)
    psum x2, waiting for transfers between devices, per_device(): hidden = lax.psum(partial_value.astype(jnp.bfloat16), 'tp')  70.6 us
    ppermute x6, waiting for transfers between devices, per_device(): lax.ppermute(ring[-1], 'sp', [(dev, (dev + 1) % 4) for dev in range(4)])  55 us
    dot_general x2, matrix products, per_device(): lax.dot_general(whole_in, current, contract_cols, preferred_element_type=...  16.9 us
    ppermute x2, waiting for transfers between devices, passed_along(): return lax.ppermute(block, axis, route)  15.7 us
    psum x2, blocking collectives, per_device(): lax.psum((jnp.sum(summed, axis=1), jnp.sum(summed * summed, axis=1)), 'tp')  13.4 us
    dot_general x2, matrix products, per_device(): lax.dot_general(scaled, lax.all_gather(out_weight[layer_index], 'sp', axi...  11.4 us
    convert_element_type x2, other arithmetic, pooled_windows(): (window_sums / counts - hidden.astype(jnp.float32)).astype(jnp.bfloat16)  8.29 us
    ppermute x2, starting transfers between devices, passed_along(): return lax.ppermute(block, axis, route)  7.08 us
  transfers between devices with their start and end apart: 12, of which 8 were waited for; matrix products, arithmetic and copies ran while one was open for 13% of the time, Pallas kernels for 0%

profile of v1, /device:TPU:0, one launch (start us, length us, event | category | flops | bytes accessed | tf_op | source)
XLA Modules:
  0.0 239.2 jit_solution(1183349852780370681)
XLA Ops:
  7.4 1.3 slice_bitcast_fusion.1
  8.6 3.1 %collective-permute-start = (bf16[256,1024]{1,0:T(8,128)(2,1)S(1)}, bf16[256,1024]{1,0:T(8,128)(2,1)S(1)}, u32[]{:S(2)}, u32[]{:S(2)}) collective-permute-start(bf16[256,1024]{1,0:T(8,128)(2,1)S(1)} %get-tuple-element.18), channel_id=1, source_target_pairs={{0,4},{4,8},{8,12},{12,0},{1,5},{5,9},{9,13},{13,1},{2,6},{6,10},{... | collective-permute-start | bytes 1572872 | tf_op jit(solution)/shard_map/ppermute | solution.py:51
  11.7 13.9 %collective-permute-done = bf16[256,1024]{1,0:T(8,128)(2,1)S(1)} collective-permute-done((bf16[256,1024]{1,0:T(8,128)(2,1)S(1)}, bf16[256,1024]{1,0:T(8,128)(2,1)S(1)}, u32[]{:S(2)}, u32[]{:S(2)}) %collective-permute-start) | collective-permute-done | bytes 524320 | tf_op jit(solution)/shard_map/ppermute | solution.py:51
  25.7 14.9 %collective-permute-done.1 = bf16[256,1024]{1,0:T(8,128)(2,1)S(1)} collective-permute-done((bf16[256,1024]{1,0:T(8,128)(2,1)S(1)}, bf16[256,1024]{1,0:T(8,128)(2,1)S(1)}, u32[]{:S(2)}, u32[]{:S(2)}) %collective-permute-start.1) | collective-permute-done | bytes 524320 | tf_op jit(solution)/shard_map/ppermute | solution.py:51
  40.6 14.1 %collective-permute-done.2 = bf16[256,1024]{1,0:T(8,128)(2,1)} collective-permute-done((bf16[256,1024]{1,0:T(8,128)(2,1)S(1)}, bf16[256,1024]{1,0:T(8,128)(2,1)}, u32[]{:S(2)}, u32[]{:S(2)}) %collective-permute-start.2) | collective-permute-done | bytes 524320 | tf_op jit(solution)/shard_map/ppermute | solution.py:51
  54.7 8.5 %fusion.38 = bf16[1024,768]{1,0:T(8,128)(2,1)} fusion(bf16[768,1024]{1,0:T(8,128)(2,1)} %param.9, s32[]{:T(128)S(6)} %select_n.85, bf16[256,1024]{1,0:T(8,128)(2,1)} %collective-permute-done.2, bf16[256,1024]{1,0:T(8,128)(2,1)S(1)} %collective-permute-done.1, bf16[256,1024]{1,0:T(8,128)(2,1)S(1)} %collective-permute-done, ...), kind=kOutput, calls=%fused_computation.68 | convolution fusion | flops 1628176384 | bytes 5242884 | tf_op jit(solution)/shard_map/dot_general | solution.py:57
  63.4 1.0 fusion.65
  64.6 12.0 %collective-permute-done.4 = bf16[256,1024]{1,0:T(8,128)(2,1)S(1)} collective-permute-done((bf16[256,1024]{1,0:T(8,128)(2,1)S(1)}, bf16[256,1024]{1,0:T(8,128)(2,1)S(1)}, u32[]{:S(2)}, u32[]{:S(2)}) %collective-permute-start.4) | collective-permute-done | bytes 524320 | tf_op jit(solution)/shard_map/ppermute | solution.py:51
  76.6 27.4 %all-reduce.5.cloned.1.call-done = bf16[1024,768]{1,0:T(8,128)(2,1)} async-done(((bf16[1024,768]{1,0:T(8,128)(2,1)}), bf16[1024,768]{1,0:T(8,128)(2,1)}) %all-reduce.5.cloned.1.call-update) | async-done | bytes 1572880 | tf_op jit(solution)/shard_map/psum | solution.py:60
  104.0 1.1 slice.138
  105.1 3.4 %collective-permute-start.3 = (bf16[1024,15]{1,0:T(8,128)(2,1)S(1)}, bf16[1024,15]{1,0:T(8,128)(2,1)S(1)}, u32[]{:S(2)}, u32[]{:S(2)}) collective-permute-start(bf16[1024,15]{1,0:T(8,128)(2,1)S(1)} %slice.138), channel_id=1, source_target_pairs={{0,4},{4,8},{8,12},{1,5},{5,9},{9,13},{2,6},{6,10},{10,14},{3,7},{... | collective-permute-start | bytes 92168 | tf_op jit(solution)/shard_map/ppermute | solution.py:17
  108.5 1.7 collective-permute-start.6
  110.2 10.5 %collective-permute-done.3 = bf16[1024,15]{1,0:T(8,128)(2,1)S(1)} collective-permute-done((bf16[1024,15]{1,0:T(8,128)(2,1)S(1)}, bf16[1024,15]{1,0:T(8,128)(2,1)S(1)}, u32[]{:S(2)}, u32[]{:S(2)}) %collective-permute-start.3) | collective-permute-done | bytes 30752 | tf_op jit(solution)/shard_map/ppermute | solution.py:17
  120.8 2.2 maximum_convert_fusion
  123.0 1.0 slice_add_fusion.5
  124.1 1.0 slice_add_fusion.4
  125.1 1.0 slice_add_fusion.3
  126.5 4.1 %fusion.1 = bf16[1024,768]{1,0:T(8,128)(2,1)S(1)} fusion(f32[1024,782]{1,0:T(8,128)S(1)} %slice_add_fusion.5, f32[1024,780]{1,0:T(8,128)S(1)} %slice_add_fusion.4, f32[1024,776]{1,0:T(8,128)S(1)} %slice_add_fusion.3, bf16[1024,768]{1,0:T(8,128)(2,1)S(1)} %copy-done, f32[1024]{0:T(1024)S(1)} %fusion.57, f32[768]{0:T(1024)S(1)} %add_convert_fusion.2, ...), kind=kLoop, calls=%fused_computation.25 | loop fusion | flops 7864320 | bytes 15739904 | tf_op jit(solution)/shard_map/convert_element_type | solution.py:38
  131.3 5.8 %fusion.64 = (f32[768]{0:T(1024)S(1)}, f32[768]{0:T(1024)S(1)}, f32[768,1024]{1,0:T(8,128)}) fusion(bf16[1024,768]{1,0:T(8,128)(2,1)S(1)} %bitcast.46, bf16[1,1024,1024]{2,1,0:T(8,128)(2,1)} %all-gather.5.cloned.1.call-done, bf16[768,1024]{1,0:T(8,128)(2,1)} %param.9), kind=kOutput, calls=%fused_computation.103 | convolution fusion | flops 1615329792 | bytes 8394752 | tf_op jit(solution)/shard_map/dot_general | solution.py:68
  137.1 7.3 %all-reduce.1 = (f32[768]{0:T(1024)S(1)}, f32[768]{0:T(1024)S(1)}) all-reduce(f32[768]{0:T(1024)S(1)} %get-tuple-element.9, f32[768]{0:T(1024)S(1)} %get-tuple-element.8), channel_id=1, replica_groups=mesh['grp'=2,'sp'=4,'tp'=4] {'tp'}, use_global_device_ids=true, to_apply=%region_4.6 | all-reduce | flops 1536 | bytes 12288 | tf_op jit(solution)/shard_map/psum | solution.py:75
  144.5 8.4 %fusion.41 = bf16[1024,768]{1,0:T(8,128)(2,1)} fusion(s32[]{:T(128)S(6)} %select_n.85, bf16[256,1024]{1,0:T(8,128)(2,1)} %collective-permute-done.6, bf16[256,1024]{1,0:T(8,128)(2,1)} %collective-permute-done.5, bf16[256,1024]{1,0:T(8,128)(2,1)} %copy-done.7, bf16[256,1024]{1,0:T(8,128)(2,1)S(1)} %get-tuple-element.19, f32[768,1024]{1,0:T(8,128)} %get-tuple-element.28, ...), kind=kOutput, calls=%fused_computation.69 | convolution fusion | flops 1632108544 | bytes 6830084 | tf_op jit(solution)/shard_map/dot_general | solution.py:57
  153.5 43.2 %all-reduce.7.cloned.1.call-done = bf16[1024,768]{1,0:T(8,128)(2,1)} async-done(((bf16[1024,768]{1,0:T(8,128)(2,1)}), bf16[1024,768]{1,0:T(8,128)(2,1)}) %all-reduce.7.cloned.1.call-update) | async-done | bytes 1572880 | tf_op jit(solution)/shard_map/psum | solution.py:60
  196.8 1.1 slice.149
  197.9 3.7 %collective-permute-start.7 = (bf16[1024,15]{1,0:T(8,128)(2,1)S(1)}, bf16[1024,15]{1,0:T(8,128)(2,1)S(1)}, u32[]{:S(2)}, u32[]{:S(2)}) collective-permute-start(bf16[1024,15]{1,0:T(8,128)(2,1)S(1)} %slice.149), channel_id=1, source_target_pairs={{0,4},{4,8},{8,12},{1,5},{5,9},{9,13},{2,6},{6,10},{10,14},{3,7},{... | collective-permute-start | bytes 92168 | tf_op jit(solution)/shard_map/ppermute | solution.py:17
  201.6 5.1 %collective-permute-done.7 = bf16[1024,15]{1,0:T(8,128)(2,1)S(1)} collective-permute-done((bf16[1024,15]{1,0:T(8,128)(2,1)S(1)}, bf16[1024,15]{1,0:T(8,128)(2,1)S(1)}, u32[]{:S(2)}, u32[]{:S(2)}) %collective-permute-start.7) | collective-permute-done | bytes 30752 | tf_op jit(solution)/shard_map/ppermute | solution.py:17
  206.7 2.2 maximum_convert_fusion.1
  208.9 1.0 slice_add_fusion.2
  212.4 4.1 %fusion.3 = bf16[1024,768]{1,0:T(8,128)(2,1)S(1)} fusion(f32[1024,782]{1,0:T(8,128)S(1)} %slice_add_fusion.2, f32[1024,780]{1,0:T(8,128)S(1)} %slice_add_fusion.1, f32[1024,776]{1,0:T(8,128)S(1)} %slice_add_fusion, bf16[1024,768]{1,0:T(8,128)(2,1)S(1)} %copy-done.1, f32[1024]{0:T(1024)S(1)} %fusion.57, f32[768]{0:T(1024)S(1)} %add_convert_fusion.2, ...), kind=kLoop, calls=%fused_computation.27 | loop fusion | flops 7864320 | bytes 15739904 | tf_op jit(solution)/shard_map/convert_element_type | solution.py:38
  216.5 1.8 multiply_convert_fusion
  218.3 5.6 %fusion.63 = (f32[768]{0:T(1024)S(1)}, f32[768]{0:T(1024)S(1)}, f32[768,1024]{1,0:T(8,128)S(1)}) fusion(bf16[1024,768]{1,0:T(8,128)(2,1)} %bitcast.45, bf16[1,1024,1024]{2,1,0:T(8,128)(2,1)} %all-gather.7.cloned.1.call-done, f32[1024]{0:T(1024)S(1)} %bitcast.52, f32[1024]{0:T(1024)S(1)} %bitcast.50, f32[768]{0:T(1024)S(1)} %get-tuple-element.27, ...), kind=kOutput, calls=%fused_computation.102 | convolution fusion | flops 1619261952 | bytes 9981952 | tf_op jit(solution)/shard_map/dot_general | solution.py:68
  224.0 6.1 %all-reduce = (f32[768]{0:T(1024)S(1)}, f32[768]{0:T(1024)S(1)}) all-reduce(f32[768]{0:T(1024)S(1)} %get-tuple-element.7, f32[768]{0:T(1024)S(1)} %get-tuple-element.6), channel_id=1, replica_groups=mesh['grp'=2,'sp'=4,'tp'=4] {'tp'}, use_global_device_ids=true, to_apply=%region_9.11 | all-reduce | flops 1536 | bytes 12288 | tf_op jit(solution)/shard_map/psum | solution.py:75
  230.1 1.7 add_convert_fusion
  (46 shorter events, 4.4 us)
Async XLA Ops:
  7.4 96.6 %all-reduce.5.cloned.1.call-start = ((), (), s32[]{:S(2)}) async-start(), calls=%async_computation | async-start | bytes 3145728 | tf_op jit(solution)/shard_map/psum | solution.py:60
  8.6 17.1 %collective-permute-start = (bf16[256,1024]{1,0:T(8,128)(2,1)S(1)}, bf16[256,1024]{1,0:T(8,128)(2,1)S(1)}, u32[]{:S(2)}, u32[]{:S(2)}) collective-permute-start(bf16[256,1024]{1,0:T(8,128)(2,1)S(1)} %get-tuple-element.18), channel_id=1, source_target_pairs={{0,4},{4,8},{8,12},{12,0},{1,5},{5,9},{9,13},{13,1},{2,6},{6,10},{... | collective-permute-start | bytes 1572872 | tf_op jit(solution)/shard_map/ppermute | solution.py:51
  25.7 14.9 %collective-permute-start.1 = (bf16[256,1024]{1,0:T(8,128)(2,1)S(1)}, bf16[256,1024]{1,0:T(8,128)(2,1)S(1)}, u32[]{:S(2)}, u32[]{:S(2)}) collective-permute-start(bf16[256,1024]{1,0:T(8,128)(2,1)S(1)} %collective-permute-done), channel_id=1, source_target_pairs={{0,4},{4,8},{8,12},{12,0},{1,5},{5,9},{9,13},{13,1},{2,6},{6,10},{... | collective-permute-start | bytes 1572872 | tf_op jit(solution)/shard_map/ppermute | solution.py:51
  40.6 14.1 %collective-permute-start.2 = (bf16[256,1024]{1,0:T(8,128)(2,1)S(1)}, bf16[256,1024]{1,0:T(8,128)(2,1)}, u32[]{:S(2)}, u32[]{:S(2)}) collective-permute-start(bf16[256,1024]{1,0:T(8,128)(2,1)S(1)} %collective-permute-done.1), channel_id=1, source_target_pairs={{0,4},{4,8},{8,12},{12,0},{1,5},{5,9},{9,13},{13,1},{2,6},{6,10},{... | collective-permute-start | bytes 1572872 | tf_op jit(solution)/shard_map/ppermute | solution.py:51
  40.6 22.8 %copy-start.2 = (bf16[2,256,1024]{2,1,0:T(8,128)(2,1)S(1)}, bf16[2,256,1024]{2,1,0:T(8,128)(2,1)}, u32[]{:S(2)}) copy-start(bf16[2,256,1024]{2,1,0:T(8,128)(2,1)} %param.11) | copy-start | bytes 3145732
  63.2 1.3 copy-start.4
  63.2 1.3 copy-start.5
  63.2 13.4 %copy-start.6 = (f32[2,1024]{1,0:T(2,128)S(1)}, f32[2,1024]{1,0:T(2,128)}, u32[]{:S(2)}) copy-start(f32[2,1024]{1,0:T(2,128)} %param.15) | copy-start | bytes 24580
  63.2 68.1 %all-gather.5.cloned.1.call-start = ((), (), s32[]{:S(2)}) async-start(), calls=%async_computation.2 | async-start | bytes 2621440 | tf_op jit(solution)/shard_map/all_gather | solution.py:70
  63.3 13.3 %collective-permute-start.4 = (bf16[256,1024]{1,0:T(8,128)(2,1)S(1)}, bf16[256,1024]{1,0:T(8,128)(2,1)S(1)}, u32[]{:S(2)}, u32[]{:S(2)}) collective-permute-start(bf16[256,1024]{1,0:T(8,128)(2,1)S(1)} %get-tuple-element.19), channel_id=1, source_target_pairs={{0,4},{4,8},{8,12},{12,0},{1,5},{5,9},{9,13},{13,1},{2,6},{6,10},{... | collective-permute-start | bytes 1572872 | tf_op jit(solution)/shard_map/ppermute | solution.py:51
  64.4 132.3 %all-reduce.7.cloned.1.call-start = ((), (), s32[]{:S(2)}) async-start(), calls=%async_computation.1 | async-start | bytes 3145728 | tf_op jit(solution)/shard_map/psum | solution.py:60
  76.6 47.5 %copy-start.7 = (bf16[256,1024]{1,0:T(8,128)(2,1)}, bf16[256,1024]{1,0:T(8,128)(2,1)S(1)}, u32[]{:S(2)}) copy-start(bf16[256,1024]{1,0:T(8,128)(2,1)S(1)} %collective-permute-done.4) | copy-start | bytes 1572868
  76.6 32.0 %collective-permute-start.5 = (bf16[256,1024]{1,0:T(8,128)(2,1)S(1)}, bf16[256,1024]{1,0:T(8,128)(2,1)}, u32[]{:S(2)}, u32[]{:S(2)}) collective-permute-start(bf16[256,1024]{1,0:T(8,128)(2,1)S(1)} %collective-permute-done.4), channel_id=1, source_target_pairs={{0,4},{4,8},{8,12},{12,0},{1,5},{5,9},{9,13},{13,1},{2,6},{6,10},{... | collective-permute-start | bytes 1572872 | tf_op jit(solution)/shard_map/ppermute | solution.py:51
  105.1 15.7 %collective-permute-start.3 = (bf16[1024,15]{1,0:T(8,128)(2,1)S(1)}, bf16[1024,15]{1,0:T(8,128)(2,1)S(1)}, u32[]{:S(2)}, u32[]{:S(2)}) collective-permute-start(bf16[1024,15]{1,0:T(8,128)(2,1)S(1)} %slice.138), channel_id=1, source_target_pairs={{0,4},{4,8},{8,12},{1,5},{5,9},{9,13},{2,6},{6,10},{10,14},{3,7},{... | collective-permute-start | bytes 92168 | tf_op jit(solution)/shard_map/ppermute | solution.py:17
  108.5 35.9 %collective-permute-start.6 = (bf16[256,1024]{1,0:T(8,128)(2,1)}, bf16[256,1024]{1,0:T(8,128)(2,1)}, u32[]{:S(2)}, u32[]{:S(2)}) collective-permute-start(bf16[256,1024]{1,0:T(8,128)(2,1)} %collective-permute-done.5), channel_id=1, source_target_pairs={{0,4},{4,8},{8,12},{12,0},{1,5},{5,9},{9,13},{13,1},{2,6},{6,10},{... | collective-permute-start | bytes 1572872 | tf_op jit(solution)/shard_map/ppermute | solution.py:51
  125.1 1.4 copy-start
  126.5 4.2 %copy-start.3 = (bf16[2,4,256,256]{3,2,1,0:T(8,128)(2,1)S(1)}, bf16[2,4,256,256]{3,2,1,0:T(8,128)(2,1)}, u32[]{:S(2)}) copy-start(bf16[2,4,256,256]{3,2,1,0:T(8,128)(2,1)} %param.12) | copy-start | bytes 3145732
  152.9 65.4 %all-gather.7.cloned.1.call-start = ((), (), s32[]{:S(2)}) async-start(), calls=%async_computation.3 | async-start | bytes 2621440 | tf_op jit(solution)/shard_map/all_gather | solution.py:70
  197.9 8.8 %collective-permute-start.7 = (bf16[1024,15]{1,0:T(8,128)(2,1)S(1)}, bf16[1024,15]{1,0:T(8,128)(2,1)S(1)}, u32[]{:S(2)}, u32[]{:S(2)}) collective-permute-start(bf16[1024,15]{1,0:T(8,128)(2,1)S(1)} %slice.149), channel_id=1, source_target_pairs={{0,4},{4,8},{8,12},{1,5},{5,9},{9,13},{2,6},{6,10},{10,14},{3,7},{... | collective-permute-start | bytes 92168 | tf_op jit(solution)/shard_map/ppermute | solution.py:17
  211.0 1.4 copy-start.1
Sparse Core Ops, SparseCore 0:
  63.4 40.6 all-reduce.4
  153.1 43.6 all-reduce.6
Sparse Core Ops, SparseCore 1:
  65.3 65.8 all-gather.4
  155.0 46.3 all-gather.6
